TPU v7x, 32 devices: a whole 2x2x4 slice. The times are simulated.
32 devices in a mesh: grp: 2 (over x), sp: 8 (over z, y), tp: 2 (over core).
Axes of the slice: x: 2, y: 2, z: 4, core: 2. Of those that a mesh axis runs over, the one named last changes fastest.
Arguments:
- resid: bfloat16 [2048, 2048], P(('grp', 'sp')), parts along dimension 0, may hold values from -6 to 6
- queries_first: bfloat16 [2048, 2048], P(('grp', 'sp'), 'tp'), parts along dimension 0, may hold values from -150 to 150
- keys_first: bfloat16 [2048, 2048], P(('grp', 'sp'), 'tp'), parts along dimension 0, may hold values from -6 to 6
- values_first: bfloat16 [2048, 2048], P(('grp', 'sp'), 'tp'), parts along dimension 0, may hold values from -6 to 6
- rel_first: float32 [16, 257], P('tp'), may hold values from -4 to 4
- post_first: float32 [2048], replicated, may hold values from 0.1 to 1.9
- out_first: bfloat16 [2048, 2048], P('tp', 'sp'), may hold values from -0.125 to 0.125
- pre_second: float32 [2048], replicated, may hold values from 0.1 to 1.9
- query_weight: bfloat16 [2048, 2048], P('sp', 'tp'), may hold values from -0.125 to 0.125
- key_weight: bfloat16 [2048, 2048], P('sp', 'tp'), may hold values from -0.125 to 0.125
- value_weight: bfloat16 [2048, 2048], P('sp', 'tp'), may hold values from -0.125 to 0.125
- rel_second: float32 [16, 257], P('tp'), may hold values from -4 to 4
- post_second: float32 [2048], replicated, may hold values from 0.1 to 1.9
- out_second: bfloat16 [2048, 2048], P('tp', 'sp'), may hold values from -0.125 to 0.125
Outputs:
- hidden_two: bfloat16 [2048, 2048], P(('grp', 'sp')), parts along dimension 0
There are 2 independent parts, one for each index of `grp`. A program takes and returns all parts, laid end to end along the dimension named above; an argument that names none is the same for every part. Nothing has to cross between parts.
All inputs are finite; a program needn't handle non-finite values.
Results may differ from a plain program's by a relative error of at most 0.017.
Values may be sent and summed in bfloat16 or wider, within the bound.
A program may use at most 128 MiB of HBM per device.

v0:
```python
import jax
import jax.numpy as jnp
from jax import lax
from jax.experimental import pallas as pl
from jax.experimental.pallas import tpu as pltpu
from jax.sharding import PartitionSpec as P

MESH = pl.DeviceIdType.MESH
BF16 = jnp.bfloat16
F32 = jnp.float32

SEG = 64
LEFT = 8
REACH = 512
REL_CLIP = 128


EPS = 1e-06
NEG_FILL = -1e30


def from_behind(value, axis, steps):
    count = lax.axis_size(axis)
    initial, last = (max(0, -steps), min(count, count - steps))
    return lax.ppermute(value, axis, [(source, source + steps) for source in range(initial, last)])


def band_bias(bias_table):
    heads_here = bias_table.shape[0]
    band = (LEFT + 1) * SEG
    length = SEG + band
    index = jnp.arange(length, dtype=jnp.int32)
    distance = jnp.where(index < band, LEFT * SEG - index, LEFT * SEG + length - index)
    slot = jnp.clip(distance, -REL_CLIP, REL_CLIP) + REL_CLIP
    onehot = (slot[:, None] == jnp.arange(2 * REL_CLIP + 1, dtype=jnp.int32)[None, :]).astype(
        jnp.float32
    )
    diagonal_values = jnp.dot(bias_table, onehot.T, precision=lax.Precision.HIGHEST)
    spread = jnp.broadcast_to(diagonal_values[:, None, :], (heads_here, SEG, length)).reshape(
        heads_here, SEG * length
    )
    return spread[:, : SEG * (length - 1)].reshape(heads_here, SEG, length - 1)[:, :, :band]


def attend_band(queries, key_rows, value_rows, bias, key_live):
    rows, width = queries.shape
    heads_here = bias.shape[0]
    head_size = width // heads_here
    blocks = rows // SEG
    query_seg = queries.reshape(blocks, SEG, heads_here, head_size)
    key_seg = key_rows.reshape(blocks + LEFT, SEG, heads_here, head_size)
    value_seg = value_rows.reshape(blocks + LEFT, SEG, heads_here, head_size)
    live_seg = key_live.reshape(blocks + LEFT, SEG)
    key_band = jnp.concatenate(
        [key_seg[earlier : earlier + blocks] for earlier in range(LEFT + 1)], axis=1
    )
    value_band = jnp.concatenate(
        [value_seg[earlier : earlier + blocks] for earlier in range(LEFT + 1)], axis=1
    )
    live_band = jnp.concatenate(
        [live_seg[earlier : earlier + blocks] for earlier in range(LEFT + 1)], axis=1
    )
    scores = jnp.einsum("nqhd,nkhd->nhqk", query_seg, key_band, preferred_element_type=jnp.float32)
    scores = scores * head_size ** (-0.5) + bias[None]
    scores = jnp.where(live_band[:, None, None, :], scores, NEG_FILL)
    largest = jnp.max(scores, axis=-1, keepdims=True)
    weights = jnp.exp(scores - largest)
    weights = (weights / jnp.sum(weights, axis=-1, keepdims=True)).astype(jnp.bfloat16)
    mixed = jnp.einsum("nhqk,nkhd->nqhd", weights, value_band, preferred_element_type=jnp.float32)
    return mixed.astype(jnp.bfloat16).reshape(rows, width)


def extend_rows(pieces, member, own_rows):
    joined = jnp.concatenate([piece[member] for piece in pieces] + [own_rows], axis=0)
    return joined


def normed(hidden, gain):
    values = hidden.astype(jnp.float32)
    scale = lax.rsqrt(jnp.mean(values * values, axis=-1, keepdims=True) + EPS)
    return (values * scale * gain).astype(jnp.bfloat16)


def residual_add(branch, residual, gain):
    values = branch.astype(jnp.float32)
    scale = lax.rsqrt(jnp.mean(values * values, axis=-1, keepdims=True) + EPS)
    return (residual.astype(jnp.float32) + values * scale * gain).astype(jnp.bfloat16)


def combine(mixed, weight, residual, gain):
    partial_rows = jnp.dot(
        mixed, lax.all_gather(weight, "sp", axis=1, tiled=True), preferred_element_type=jnp.float32
    )
    branch = lax.psum_scatter(
        partial_rows.astype(jnp.bfloat16), "tp", scatter_dimension=0, tiled=True
    )
    return residual_add(branch, residual, gain)


def full_rows(share):
    return lax.all_gather(share, "tp", axis=0, tiled=True)


def shards(
    resid,
    queries_first,
    keys_first,
    values_first,
    rel_first,
    post_first,
    out_first,
    pre_second,
    query_weight,
    key_weight,
    value_weight,
    rel_second,
    post_second,
    out_second,
):
    tok_rows = resid.shape[0]
    n_sp = lax.axis_size("sp")
    if (
        rel_first.shape[0] == n_sp
        and n_sp % 2 == 0
        and lax.axis_size("tp") == 2
        and lax.axis_size("grp") == 2
        and REACH % tok_rows == 0
        and tok_rows == REL_CLIP
    ):
        return by_heads(
            resid, queries_first, keys_first, values_first, rel_first, post_first, out_first,
            pre_second, query_weight, key_weight, value_weight, rel_second, post_second, out_second,
        )
    depth = (REACH + tok_rows - 1) // tok_rows
    anchor = lax.axis_index("sp") * tok_rows
    key_live = anchor - REACH + jnp.arange(tok_rows + REACH, dtype=jnp.int32) >= 0
    share_rows = tok_rows // lax.axis_size("tp")
    base_rows = lax.dynamic_slice_in_dim(resid, lax.axis_index("tp") * share_rows, share_rows, 0)
    earlier_first = [
        from_behind((keys_first, values_first), "sp", distance) for distance in range(depth, 0, -1)
    ]
    key_ext = extend_rows(earlier_first, 0, keys_first)
    value_ext = extend_rows(earlier_first, 1, values_first)
    first = attend_band(queries_first, key_ext, value_ext, band_bias(rel_first), key_live)
    hidden_one = combine(first, out_first, base_rows, post_first)
    inputs_two = full_rows(normed(hidden_one, pre_second))
    query_sum = jnp.dot(
        inputs_two,
        lax.all_gather(query_weight, "sp", axis=0, tiled=True),
        preferred_element_type=jnp.float32,
    )
    key_sum = jnp.dot(
        inputs_two,
        lax.all_gather(key_weight, "sp", axis=0, tiled=True),
        preferred_element_type=jnp.float32,
    )
    value_sum = jnp.dot(
        inputs_two,
        lax.all_gather(value_weight, "sp", axis=0, tiled=True),
        preferred_element_type=jnp.float32,
    )
    queries_two = query_sum.astype(jnp.bfloat16)
    keys_two = key_sum.astype(jnp.bfloat16)
    values_two = value_sum.astype(jnp.bfloat16)
    earlier_second = [
        from_behind((keys_two, values_two), "sp", distance) for distance in range(depth, 0, -1)
    ]
    key_ext_two = extend_rows(earlier_second, 0, keys_two)
    value_ext_two = extend_rows(earlier_second, 1, values_two)
    second = attend_band(queries_two, key_ext_two, value_ext_two, band_bias(rel_second), key_live)
    hidden_two = combine(second, out_second, hidden_one, post_second)
    return full_rows(hidden_two)


def scaled(values):
    return values * lax.rsqrt(jnp.mean(values * values, axis=-1, keepdims=True) + EPS)


def build_kernel(n, tok, head, width, reach):
    share = tok // 2
    cols = width // n
    span = reach + tok
    model = width

    def kernel(
        q_hbm, k_hbm, v_hbm, wq_hbm, wk_hbm, wv_hbm, resid_hbm, o1_hbm, o2_hbm,
        rel1, rel2, post1, pre2, post2,
        out_ref,
        heads, weights, outs, res, bias, mixed1, mixed2, parts, inbox, joined, branch, rows2, total, last,
        loc_sem, hs, hr, ws, wr, wf, fs, fr, gs, gr, ps, pr, bs, br, xs, xr, ys, yr,
    ):
        s = lax.axis_index("sp")
        t = lax.axis_index("tp")
        g = lax.axis_index("grp")
        u = 1 - t
        side = s + 1 - 2 * lax.rem(s, 2)

        def rcopy(src, dst, ssem, rsem, sp, tp, grp=g):
            return pltpu.make_async_remote_copy(
                src_ref=src, dst_ref=dst, send_sem=ssem, recv_sem=rsem,
                device_id={"grp": grp, "sp": sp, "tp": tp}, device_id_type=MESH,
            )

        def peer(k):
            return lax.rem(s + k, n)

        barrier = pltpu.get_barrier_semaphore()
        for k in range(n):
            if k:
                pl.semaphore_signal(
                    barrier, inc=1, device_id={"sp": peer(k), "tp": t}, device_id_type=MESH
                )
            pl.semaphore_signal(
                barrier, inc=1, device_id={"sp": peer(k), "tp": u}, device_id_type=MESH
            )
        pl.semaphore_signal(
            barrier, inc=1, device_id={"grp": 1 - g, "sp": s, "tp": t}, device_id_type=MESH
        )
        pl.semaphore_wait(barrier, 2 * n)

        def lanes(j):
            return pl.ds(pl.multiple_of(j * head, head), head)

        def trows(j, base=0):
            return pl.ds(pl.multiple_of(base + j * tok, tok), tok)

        wrows = width // n

        def head_copy(i, ref, j, src):
            dst = heads.at[i, trows(src, reach)]
            return rcopy(ref.at[:, lanes(j)], dst, hs.at[i, j], hr.at[i, src], j, t)

        hrows = wrows // 2

        def weight_half(i, src, part):
            start = pl.multiple_of(src * wrows + part * hrows, hrows)
            return weights.at[pl.ds(start, hrows), pl.ds(i * head, head)]

        def weight_copy(i, j, src):
            piece = wqkv[i].at[pl.ds(pl.multiple_of(g * hrows, hrows), hrows), lanes(j)]
            return rcopy(piece, weight_half(i, src, g), ws.at[i, j], wr.at[i, src, g], j, t)

        def weight_hand(i, src):
            piece = weight_half(i, src, g)
            return rcopy(piece, piece, wf.at[i, src], wr.at[i, src, g], s, t, 1 - g)

        def weight_handed(i, src):
            piece = weight_half(i, src, 1 - g)
            return rcopy(piece, piece, wf.at[i, src], wr.at[i, src, 1 - g], s, t, 1 - g)

        def own_weights(i):
            return pltpu.make_async_copy(
                wqkv[i].at[:, lanes(s)],
                weights.at[pl.ds(pl.multiple_of(s * wrows, wrows), wrows), pl.ds(i * head, head)],
                wr.at[i, s, 0],
            )

        qkv = (q_hbm, k_hbm, v_hbm)
        wqkv = (wq_hbm, wk_hbm, wv_hbm)
        for k in range(1, n):
            for i in range(3):
                head_copy(i, qkv[i], peer(k), s).start()
        for i in range(3):
            pltpu.make_async_copy(
                qkv[i].at[:, lanes(s)], heads.at[i, trows(s, reach)], hr.at[i, s]
            ).start()
        for i in range(3):
            own_weights(i).start()

        def send_weights():
            for i in range(3):
                for k in range(1, n):
                    weight_copy(i, peer(k), s).start()

        local = [
            pltpu.make_async_copy(o1_hbm, outs.at[0], loc_sem.at[0]),
            pltpu.make_async_copy(o2_hbm, outs.at[1], loc_sem.at[1]),
            pltpu.make_async_copy(
                resid_hbm.at[pl.ds(pl.multiple_of(t * share, share), share)], res, loc_sem.at[2]
            ),
        ]
        for copy in local:
            copy.start()

        near = 2 * REL_CLIP
        query = lax.broadcasted_iota(jnp.int32, (tok, span), 0) // SEG
        key = lax.broadcasted_iota(jnp.int32, (tok, span), 1) // SEG
        live = (key >= query) & (key <= query + LEFT)
        for layer, rel in enumerate((rel1, rel2)):
            table = rel[pl.ds(s, 1), :]
            top = table[:, near : near + 1]
            entry = lax.broadcasted_iota(jnp.int32, (near, near + tok), 0)
            place = lax.broadcasted_iota(jnp.int32, (near, near + tok), 1)
            flip = (entry + place == near).astype(F32)
            line = jnp.dot(
                jnp.broadcast_to(table[:, :near], (8, near)), flip,
                preferred_element_type=F32, precision=lax.Precision.HIGHEST,
            )[:1]
            spot = lax.broadcasted_iota(jnp.int32, line.shape, 1)
            line = jnp.where((spot == 0) | (spot >= near), top, line)
            spread = jnp.broadcast_to(line, (tok, near + tok))
            row = lax.broadcasted_iota(jnp.int32, spread.shape, 0)
            step = 1
            while step < tok:
                moved = pltpu.roll(spread, step, 1)
                spread = jnp.where(lax.rem(row // step, 2) == 1, moved, spread)
                step *= 2
            far = jnp.broadcast_to(top, (tok, span - near))
            whole = jnp.concatenate([far, spread[:, :near]], axis=1)
            bias[layer] = jnp.where(live, whole, NEG_FILL)

        heads[1, :reach] = jnp.zeros((reach, head), BF16)
        heads[2, :reach] = jnp.zeros((reach, head), BF16)

        def attend(layer, b):
            q = heads[0, trows(b, reach)]
            k = heads[1, pl.ds(pl.multiple_of(b * tok, tok), span)]
            v = heads[2, pl.ds(pl.multiple_of(b * tok, tok), span)]
            scores = lax.dot_general(
                q, k, (((1,), (1,)), ((), ())), preferred_element_type=F32
            ) * head ** (-0.5) + bias[layer]
            column = lax.broadcasted_iota(jnp.int32, scores.shape, 1)
            scores = jnp.where(column >= reach - b * tok, scores, NEG_FILL)
            e = jnp.exp(scores - jnp.max(scores, axis=-1, keepdims=True))
            e = (e * (1.0 / jnp.sum(e, axis=-1, keepdims=True))).astype(BF16)
            return jnp.dot(e, v, preferred_element_type=F32).astype(BF16)

        def layer_branch(layer, mixed, ms, mr, wait_block, after_own):
            def mcopy(b, src, k, sp):
                block = mixed.at[src, trows(b)]
                return rcopy(block, block, ms.at[b, k], mr.at[b, src], sp, t)

            half = n // 2

            def forward(b):
                for k in range(1, half):
                    mcopy(b, peer(2 * k), k, side).wait_recv()
                    mcopy(b, peer(2 * k), half - 1 + k, side).start()

            def own(b, _):
                wait_block(b)
                mixed[s, trows(b)] = attend(layer, b)
                mcopy(b, s, 0, side).start()
                for k in range(1, half):
                    mcopy(b, s, k, peer(2 * k)).start()

                @pl.when(b >= half)
                def _():
                    forward(b - half)

                return 0

            lax.fori_loop(0, n, own, 0)
            after_own()

            def pcopy(b):
                return rcopy(
                    parts.at[layer, b, u], inbox.at[layer, b],
                    ps.at[layer, b], pr.at[layer, b], s, u,
                )

            def bcopy(b, src):
                return rcopy(
                    joined.at[layer, b], branch.at[layer, src],
                    bs.at[layer, b], br.at[layer, src], b, t,
                )

            def project(b):
                for k in range(half):
                    mcopy(b, lax.rem(side + 2 * k, n), k, side).wait_recv()
                lhs = jnp.concatenate([mixed[j, trows(b)] for j in range(n)], axis=1)
                part = jnp.dot(lhs, outs[layer], preferred_element_type=F32).astype(BF16)
                parts[layer, b, 0] = part[:share]
                parts[layer, b, 1] = part[share:]
                pcopy(b).start()

            def join(b):
                pcopy(b).wait_recv()
                both = parts[layer, b, t].astype(F32) + inbox[layer, b].astype(F32)
                joined[layer, b] = both.astype(BF16)

                @pl.when(b != s)
                def _():
                    bcopy(b, s).start()

                @pl.when(b == s)
                def _():
                    pltpu.make_async_copy(
                        joined.at[layer, b], branch.at[layer, s], br.at[layer, s]
                    ).start()

            def step(b, _):
                @pl.when(b < half)
                def _():
                    forward(n - half + b)

                project(b)

                @pl.when(b > 0)
                def _():
                    join(b - 1)

                return 0

            lax.fori_loop(0, n, step, 0)
            join(n - 1)

            def arrived(j, _):
                bcopy(side, j).wait_recv()
                return 0

            lax.fori_loop(0, n, arrived, 0)

            def drain(b, _):
                for k in range(2 * half - 1):
                    mcopy(b, s, k, side).wait_send()
                pcopy(b).wait_send()

                @pl.when(b != s)
                def _():
                    bcopy(b, s).wait_send()

                return 0

            values = jnp.concatenate([branch[layer, j] for j in range(n)], axis=1)
            return values.astype(F32), drain

        def heads_ready(b):
            for i in range(3):
                head_copy(i, qkv[i], side, b).wait_recv()

        local[0].wait()
        local[1].wait()
        values, drain1 = layer_branch(0, mixed1, fs, fr, heads_ready, send_weights)
        local[2].wait()
        hidden = (res[...].astype(F32) + scaled(values) * post1[...]).astype(BF16)
        res[...] = hidden
        rows2[2 * s + t] = (scaled(hidden.astype(F32)) * pre2[...]).astype(BF16)

        half = n // 2
        wide = width // half

        def xcopy(src, c, k, sp, tp, m):
            block = rows2.at[2 * src + c, :, pl.ds(pl.multiple_of(m * wide, wide), wide)]
            return rcopy(block, block, xs.at[src, k, m], xr.at[2 * src + c, m], sp, tp)

        def xsend(m, _):
            for k in range(1, half):
                xcopy(s, t, k + 1, peer(2 * k), t, m).start()
            xcopy(s, t, 0, side, t, m).start()
            xcopy(s, t, 1, s, u, m).start()
            return 0

        lax.fori_loop(0, half, xsend, 0)

        def hand_weights(k, _):
            for i in range(3):
                weight_copy(i, side, peer(k)).wait_recv()
                weight_hand(i, peer(k)).start()
            return 0

        lax.fori_loop(1, n, hand_weights, 0)

        def near_rows(m, _):
            for k in range(1, half):
                src = peer(2 * k)
                xcopy(src, t, 0, side, t, m).wait_recv()
                xcopy(src, t, 0, side, t, m).start()
                xcopy(src, t, 1, s, u, m).start()
            return 0

        lax.fori_loop(0, half, near_rows, 0)

        def weights_ready(k, _):
            for i in range(3):
                weight_handed(i, peer(k)).wait_recv()
            return 0

        lax.fori_loop(1, n, weights_ready, 0)
        for i in range(3):
            own_weights(i).wait()

        def project_rows(m):
            for src in range(n):
                xcopy(src, u, 1, s, u, m).wait_recv()
            depth = pl.ds(pl.multiple_of(m * wide, wide), wide)
            lhs = rows2[:, :, depth].reshape(n * tok, wide)
            total[...] += jnp.dot(lhs, weights[depth, :], preferred_element_type=F32)

        total[...] = jnp.zeros_like(total)

        def far_rows(m, _):
            for k in range(half):
                src = lax.rem(side + 2 * k, n)
                xcopy(src, t, 0, side, t, m).wait_recv()
                xcopy(src, t, 1, s, u, m).start()

            @pl.when(m > 0)
            def _():
                project_rows(m - 1)

            return 0

        lax.fori_loop(0, half, far_rows, 0)
        project_rows(half - 1)
        for i in range(3):
            heads[i, reach:] = total[:, i * head : (i + 1) * head].astype(BF16)

        values, drain2 = layer_branch(1, mixed2, gs, gr, lambda b: None, lambda: None)
        done = (res[...].astype(F32) + scaled(values) * post2[...]).astype(BF16)
        last[t] = done
        final = rcopy(last.at[t], last.at[t], ys, yr, s, u)
        final.start()

        lax.fori_loop(0, n, lambda b, c: drain1(b, c), 0)
        lax.fori_loop(0, n, lambda b, c: drain2(b, c), 0)
        def drain_first(k, _):
            for i in range(3):
                head_copy(i, qkv[i], peer(k), s).wait_send()
                weight_copy(i, peer(k), s).wait_send()
                weight_hand(i, peer(k)).wait_send()
            return 0

        lax.fori_loop(1, n, drain_first, 0)

        def drain_rows(m, _):
            for k in range(half + 1):
                xcopy(s, t, k, side, t, m).wait_send()
            for k in range(1, half):
                xcopy(peer(2 * k), t, 0, side, t, m).wait_send()
                xcopy(peer(2 * k), t, 1, side, t, m).wait_send()
            for k in range(half):
                xcopy(lax.rem(side + 2 * k, n), t, 1, side, t, m).wait_send()
            return 0

        lax.fori_loop(0, half, drain_rows, 0)
        final.wait_send()
        rcopy(last.at[u], last.at[u], ys, yr, s, u).wait_recv()
        out_ref[:share] = last[0]
        out_ref[share:] = last[1]

    half = n // 2
    scratch = [
        pltpu.VMEM((3, reach + n * tok, head), BF16),
        pltpu.VMEM((width, 3 * head), BF16),
        pltpu.VMEM((2, n * head, cols), BF16),
        pltpu.VMEM((share, width), BF16),
        pltpu.VMEM((2, tok, span), F32),
        pltpu.VMEM((n, n * tok, head), BF16),
        pltpu.VMEM((n, n * tok, head), BF16),
        pltpu.VMEM((2, n, 2, share, cols), BF16),
        pltpu.VMEM((2, n, share, cols), BF16),
        pltpu.VMEM((2, n, share, cols), BF16),
        pltpu.VMEM((2, n, share, cols), BF16),
        pltpu.VMEM((2 * n, share, width), BF16),
        pltpu.VMEM((n * tok, 3 * head), F32),
        pltpu.VMEM((2, share, width), BF16),
        pltpu.SemaphoreType.DMA((3,)),
        pltpu.SemaphoreType.DMA((3, n)),
        pltpu.SemaphoreType.DMA((3, n)),
        pltpu.SemaphoreType.DMA((3, n)),
        pltpu.SemaphoreType.DMA((3, n, 2)),
        pltpu.SemaphoreType.DMA((3, n)),
        pltpu.SemaphoreType.DMA((n, 2 * half - 1)),
        pltpu.SemaphoreType.DMA((n, n)),
        pltpu.SemaphoreType.DMA((n, 2 * half - 1)),
        pltpu.SemaphoreType.DMA((n, n)),
        pltpu.SemaphoreType.DMA((2, n)),
        pltpu.SemaphoreType.DMA((2, n)),
        pltpu.SemaphoreType.DMA((2, n)),
        pltpu.SemaphoreType.DMA((2, n)),
        pltpu.SemaphoreType.DMA((n, half + 1, half)),
        pltpu.SemaphoreType.DMA((2 * n, half)),
        pltpu.SemaphoreType.DMA,
        pltpu.SemaphoreType.DMA,
    ]
    return kernel, scratch


def by_heads(
    resid, queries_first, keys_first, values_first, rel_first, post_first, out_first, pre_second,
    query_weight, key_weight, value_weight, rel_second, post_second, out_second,
):
    n = lax.axis_size("sp")
    tok, width = resid.shape
    head = queries_first.shape[1] // rel_first.shape[0]
    kernel, scratch = build_kernel(n, tok, head, width, REACH)
    hbm = pl.BlockSpec(memory_space=pltpu.HBM)
    vmem = pl.BlockSpec(memory_space=pltpu.VMEM)
    return pl.pallas_call(
        kernel,
        out_shape=jax.ShapeDtypeStruct((tok, width), BF16),
        in_specs=[hbm] * 9 + [vmem] * 5,
        out_specs=vmem,
        scratch_shapes=scratch,
        compiler_params=pltpu.CompilerParams(
            collective_id=0, has_side_effects=True, vmem_limit_bytes=60 * 2**20
        ),
    )(
        queries_first, keys_first, values_first, query_weight, key_weight, value_weight, resid,
        out_first, out_second, rel_first, rel_second,
        post_first[None], pre_second[None], post_second[None],
    )


def solution(mesh):
    in_specs = (
        P(("grp", "sp"), None),
        P(("grp", "sp"), "tp"),
        P(("grp", "sp"), "tp"),
        P(("grp", "sp"), "tp"),
        P("tp", None),
        P(),
        P("tp", "sp"),
        P(),
        P("sp", "tp"),
        P("sp", "tp"),
        P("sp", "tp"),
        P("tp", None),
        P(),
        P("tp", "sp"),
    )
    out_specs = P(("grp", "sp"), None)
    return jax.shard_map(shards, mesh=mesh, in_specs=in_specs, out_specs=out_specs, check_vma=False)
```

profile of v0, /device:TPU:27, one launch (start us, length us, event | category | flops | bytes accessed | tf_op | source)
XLA Modules:
  0.0 144.6 jit_solution(12143424357266452576)
XLA Ops:
  0.0 142.7 %shard_map.136 = bf16[128,2048]{1,0:T(8,128)(2,1)} custom-call(bf16[128,1024]{1,0:T(8,128)(2,1)} %q_hbm.1, bf16[128,1024]{1,0:T(8,128)(2,1)} %k_hbm.1, bf16[128,1024]{1,0:T(8,128)(2,1)} %v_hbm.1, bf16[256,1024]{1,0:T(8,128)(2,1)} %wq_hbm.1, bf16[256,1024]{1,0:T(8,128)(2,1)} %wk_hbm.1, bf16[256,1024]{1,0:T(8,128)(2,1)} %wv_hbm.1, ...), custom_call_target="tpu_custom_call" | custom-call | tf_op jit(solution)/shard_map/pallas_call | solution.py:590
  142.8 1.9 %copy.16 = bf16[128,2048]{1,0:T(8,128)(2,1)} copy(bf16[128,2048]{1,0:T(8,128)(2,1)} %shard_map.136) | data formatting | bytes 1048576
where the time goes:
time: 145 us
  Pallas kernels  143 us (99%)
  local copies, waits for them, and re-layouts  1.88 us (1%)
    pallas_call x1, Pallas kernels, by_heads(): pl.pallas_call(kernel, out_shape=jax.ShapeDtypeStruct((tok, width), BF16)...  143 us

commit v1 on v0

v1 whole, which is shorter than its diff:
```python
import jax
import jax.numpy as jnp
from jax import lax
from jax.experimental import pallas as pl
from jax.experimental.pallas import tpu as pltpu
from jax.sharding import PartitionSpec as P

MESH = pl.DeviceIdType.MESH
BF16 = jnp.bfloat16
F32 = jnp.float32

SEG = 64
LEFT = 8
REACH = 512
REL_CLIP = 128


EPS = 1e-06
NEG_FILL = -1e30


def from_behind(value, axis, steps):
    count = lax.axis_size(axis)
    initial, last = (max(0, -steps), min(count, count - steps))
    return lax.ppermute(value, axis, [(source, source + steps) for source in range(initial, last)])


def band_bias(bias_table):
    heads_here = bias_table.shape[0]
    band = (LEFT + 1) * SEG
    length = SEG + band
    index = jnp.arange(length, dtype=jnp.int32)
    distance = jnp.where(index < band, LEFT * SEG - index, LEFT * SEG + length - index)
    slot = jnp.clip(distance, -REL_CLIP, REL_CLIP) + REL_CLIP
    onehot = (slot[:, None] == jnp.arange(2 * REL_CLIP + 1, dtype=jnp.int32)[None, :]).astype(
        jnp.float32
    )
    diagonal_values = jnp.dot(bias_table, onehot.T, precision=lax.Precision.HIGHEST)
    spread = jnp.broadcast_to(diagonal_values[:, None, :], (heads_here, SEG, length)).reshape(
        heads_here, SEG * length
    )
    return spread[:, : SEG * (length - 1)].reshape(heads_here, SEG, length - 1)[:, :, :band]


def attend_band(queries, key_rows, value_rows, bias, key_live):
    rows, width = queries.shape
    heads_here = bias.shape[0]
    head_size = width // heads_here
    blocks = rows // SEG
    query_seg = queries.reshape(blocks, SEG, heads_here, head_size)
    key_seg = key_rows.reshape(blocks + LEFT, SEG, heads_here, head_size)
    value_seg = value_rows.reshape(blocks + LEFT, SEG, heads_here, head_size)
    live_seg = key_live.reshape(blocks + LEFT, SEG)
    key_band = jnp.concatenate(
        [key_seg[earlier : earlier + blocks] for earlier in range(LEFT + 1)], axis=1
    )
    value_band = jnp.concatenate(
        [value_seg[earlier : earlier + blocks] for earlier in range(LEFT + 1)], axis=1
    )
    live_band = jnp.concatenate(
        [live_seg[earlier : earlier + blocks] for earlier in range(LEFT + 1)], axis=1
    )
    scores = jnp.einsum("nqhd,nkhd->nhqk", query_seg, key_band, preferred_element_type=jnp.float32)
    scores = scores * head_size ** (-0.5) + bias[None]
    scores = jnp.where(live_band[:, None, None, :], scores, NEG_FILL)
    largest = jnp.max(scores, axis=-1, keepdims=True)
    weights = jnp.exp(scores - largest)
    weights = (weights / jnp.sum(weights, axis=-1, keepdims=True)).astype(jnp.bfloat16)
    mixed = jnp.einsum("nhqk,nkhd->nqhd", weights, value_band, preferred_element_type=jnp.float32)
    return mixed.astype(jnp.bfloat16).reshape(rows, width)


def extend_rows(pieces, member, own_rows):
    joined = jnp.concatenate([piece[member] for piece in pieces] + [own_rows], axis=0)
    return joined


def normed(hidden, gain):
    values = hidden.astype(jnp.float32)
    scale = lax.rsqrt(jnp.mean(values * values, axis=-1, keepdims=True) + EPS)
    return (values * scale * gain).astype(jnp.bfloat16)


def residual_add(branch, residual, gain):
    values = branch.astype(jnp.float32)
    scale = lax.rsqrt(jnp.mean(values * values, axis=-1, keepdims=True) + EPS)
    return (residual.astype(jnp.float32) + values * scale * gain).astype(jnp.bfloat16)


def combine(mixed, weight, residual, gain):
    partial_rows = jnp.dot(
        mixed, lax.all_gather(weight, "sp", axis=1, tiled=True), preferred_element_type=jnp.float32
    )
    branch = lax.psum_scatter(
        partial_rows.astype(jnp.bfloat16), "tp", scatter_dimension=0, tiled=True
    )
    return residual_add(branch, residual, gain)


def full_rows(share):
    return lax.all_gather(share, "tp", axis=0, tiled=True)


def shards(
    resid,
    queries_first,
    keys_first,
    values_first,
    rel_first,
    post_first,
    out_first,
    pre_second,
    query_weight,
    key_weight,
    value_weight,
    rel_second,
    post_second,
    out_second,
):
    tok_rows = resid.shape[0]
    n_sp = lax.axis_size("sp")
    if (
        rel_first.shape[0] == n_sp
        and n_sp % 2 == 0
        and lax.axis_size("tp") == 2
        and lax.axis_size("grp") == 2
        and REACH % tok_rows == 0
        and tok_rows == REL_CLIP
    ):
        return by_heads(
            resid, queries_first, keys_first, values_first, rel_first, post_first, out_first,
            pre_second, query_weight, key_weight, value_weight, rel_second, post_second, out_second,
        )
    depth = (REACH + tok_rows - 1) // tok_rows
    anchor = lax.axis_index("sp") * tok_rows
    key_live = anchor - REACH + jnp.arange(tok_rows + REACH, dtype=jnp.int32) >= 0
    share_rows = tok_rows // lax.axis_size("tp")
    base_rows = lax.dynamic_slice_in_dim(resid, lax.axis_index("tp") * share_rows, share_rows, 0)
    earlier_first = [
        from_behind((keys_first, values_first), "sp", distance) for distance in range(depth, 0, -1)
    ]
    key_ext = extend_rows(earlier_first, 0, keys_first)
    value_ext = extend_rows(earlier_first, 1, values_first)
    first = attend_band(queries_first, key_ext, value_ext, band_bias(rel_first), key_live)
    hidden_one = combine(first, out_first, base_rows, post_first)
    inputs_two = full_rows(normed(hidden_one, pre_second))
    query_sum = jnp.dot(
        inputs_two,
        lax.all_gather(query_weight, "sp", axis=0, tiled=True),
        preferred_element_type=jnp.float32,
    )
    key_sum = jnp.dot(
        inputs_two,
        lax.all_gather(key_weight, "sp", axis=0, tiled=True),
        preferred_element_type=jnp.float32,
    )
    value_sum = jnp.dot(
        inputs_two,
        lax.all_gather(value_weight, "sp", axis=0, tiled=True),
        preferred_element_type=jnp.float32,
    )
    queries_two = query_sum.astype(jnp.bfloat16)
    keys_two = key_sum.astype(jnp.bfloat16)
    values_two = value_sum.astype(jnp.bfloat16)
    earlier_second = [
        from_behind((keys_two, values_two), "sp", distance) for distance in range(depth, 0, -1)
    ]
    key_ext_two = extend_rows(earlier_second, 0, keys_two)
    value_ext_two = extend_rows(earlier_second, 1, values_two)
    second = attend_band(queries_two, key_ext_two, value_ext_two, band_bias(rel_second), key_live)
    hidden_two = combine(second, out_second, hidden_one, post_second)
    return full_rows(hidden_two)


def scaled(values):
    return values * lax.rsqrt(jnp.mean(values * values, axis=-1, keepdims=True) + EPS)


def build_kernel(n, tok, head, width, reach):
    share = tok // 2
    cols = width // n
    span = reach + tok
    levels = n // 2
    depth = n * head
    dhalf = depth // 2
    wrows = width // n
    hrows = wrows // 2
    pieces = 4
    wide = width // pieces

    def kernel(
        q_hbm, k_hbm, v_hbm, wq_hbm, wk_hbm, wv_hbm, resid_hbm, o1_hbm, o2_hbm,
        rel1, rel2, post1, pre2, post2,
        out_ref,
        heads, weights, outs, res, bias, own_mix, mixed, parts, inbox, joined, branch, rows2, last,
        loc_sem, hs, hr, ws, wr, wf, mzs, mzr, mys, myr, ozs, ozr, oxs, oxr,
        ps, pr, bs, br, rzs, rzr, rys, ryr, rds, rdr, fs, fr,
    ):
        s = lax.axis_index("sp")
        t = lax.axis_index("tp")
        g = lax.axis_index("grp")
        u = 1 - t
        z = s // 2
        y = lax.rem(s, 2)
        v = 1 - y
        side = 2 * z + v
        turn = 1 - 2 * lax.rem(z, 2)

        def rcopy(src, dst, ssem, rsem, sp, tp, grp=g):
            return pltpu.make_async_remote_copy(
                src_ref=src, dst_ref=dst, send_sem=ssem, recv_sem=rsem,
                device_id={"grp": grp, "sp": sp, "tp": tp}, device_id_type=MESH,
            )

        def peer(k):
            return lax.rem(s + k, n)

        def near_level(i):
            return lax.rem(z + turn * i + levels, levels)

        def arrived(ref, sem):
            pltpu.make_async_copy(ref, ref, sem).wait()

        barrier = pltpu.get_barrier_semaphore()
        for k in range(1, n):
            pl.semaphore_signal(
                barrier, inc=1, device_id={"grp": g, "sp": peer(k), "tp": t}, device_id_type=MESH
            )
        pl.semaphore_signal(
            barrier, inc=1, device_id={"grp": g, "sp": s, "tp": u}, device_id_type=MESH
        )
        pl.semaphore_signal(
            barrier, inc=1, device_id={"grp": 1 - g, "sp": s, "tp": t}, device_id_type=MESH
        )
        pl.semaphore_wait(barrier, n + 1)

        def lanes(j):
            return pl.ds(pl.multiple_of(j * head, head), head)

        def trows(j, base=0):
            return pl.ds(pl.multiple_of(base + j * tok, tok), tok)

        qkv = (q_hbm, k_hbm, v_hbm)
        wqkv = (wq_hbm, wk_hbm, wv_hbm)
        out_hbm = (o1_hbm, o2_hbm)

        def head_copy(i, j):
            dst = heads.at[i, trows(s, reach)]
            return rcopy(qkv[i].at[:, lanes(j)], dst, hs, hr.at[s], j, t)

        def weight_half(src, part):
            start = pl.multiple_of(src * wrows + part * hrows, hrows)
            return weights.at[pl.ds(start, hrows)]

        def weight_copy(i, j):
            start = pl.multiple_of(s * wrows + g * hrows, hrows)
            piece = wqkv[i].at[pl.ds(pl.multiple_of(g * hrows, hrows), hrows), lanes(j)]
            dst = weights.at[pl.ds(start, hrows), pl.ds(i * head, head)]
            return rcopy(piece, dst, ws, wr.at[s, g], j, t)

        def weight_hand(src):
            piece = weight_half(src, g)
            return rcopy(piece, piece, wf, wr.at[src, g], s, t, 1 - g)

        def out_half(layer, c, part):
            return outs.at[layer, c, pl.ds(pl.multiple_of(part * dhalf, dhalf), dhalf)]

        def out_own(layer, to):
            piece = out_hbm[layer].at[pl.ds(pl.multiple_of(g * dhalf, dhalf), dhalf)]
            return rcopy(
                piece, out_half(layer, z, g), ozs.at[layer], ozr.at[layer, z], 2 * to + y, t
            )

        def out_pass(layer, c, to):
            piece = out_half(layer, c, g)
            return rcopy(piece, piece, ozs.at[layer], ozr.at[layer, c], 2 * to + y, t)

        def out_hand(layer, c):
            piece = out_half(layer, c, g)
            return rcopy(piece, piece, oxs.at[layer], oxr.at[layer, c], s, t, 1 - g)

        def out_start(layer):
            @pl.when(z < levels - 1)
            def _():
                out_own(layer, z + 1).start()

            @pl.when(z > 0)
            def _():
                out_own(layer, z - 1).start()

        def out_hop(layer, d):
            @pl.when(z >= d)
            def _():
                arrived(out_half(layer, z - d, g), ozr.at[layer, z - d])

                @pl.when(z < levels - 1)
                def _():
                    out_pass(layer, z - d, z + 1).start()

                out_hand(layer, z - d).start()

            @pl.when(z + d < levels)
            def _():
                arrived(out_half(layer, z + d, g), ozr.at[layer, z + d])

                @pl.when(z > 0)
                def _():
                    out_pass(layer, z + d, z - 1).start()

                out_hand(layer, z + d).start()

        def out_drain(layer):
            for at in range(levels):
                count = (1 + at if at < levels - 1 else 0) + (levels - at if at > 0 else 0)
                block = rows2.at[pl.ds(0, count)]

                @pl.when(z == at)
                def _():
                    arrived(block, ozs.at[layer])

            arrived(rows2.at[pl.ds(0, levels - 1)], oxs.at[layer])

        out_start(0)
        for k in range(1, n):
            for i in range(3):
                head_copy(i, peer(k)).start()
        for i in range(3):
            pltpu.make_async_copy(
                qkv[i].at[:, lanes(s)], heads.at[i, trows(s, reach)], hr.at[s]
            ).start()
        for i in range(3):
            pltpu.make_async_copy(
                wqkv[i].at[:, lanes(s)],
                weights.at[pl.ds(pl.multiple_of(s * wrows, wrows), wrows), pl.ds(i * head, head)],
                wr.at[s, 0],
            ).start()
        local = [
            pltpu.make_async_copy(o1_hbm, outs.at[0, z], loc_sem.at[0]),
            pltpu.make_async_copy(o2_hbm, outs.at[1, z], loc_sem.at[1]),
            pltpu.make_async_copy(
                resid_hbm.at[pl.ds(pl.multiple_of(t * share, share), share)], res, loc_sem.at[2]
            ),
        ]
        for copy in local:
            copy.start()

        near = 2 * REL_CLIP
        query = lax.broadcasted_iota(jnp.int32, (tok, span), 0) // SEG
        key = lax.broadcasted_iota(jnp.int32, (tok, span), 1) // SEG
        live = (key >= query) & (key <= query + LEFT)
        for layer, rel in enumerate((rel1, rel2)):
            table = rel[pl.ds(s, 1), :]
            top = table[:, near : near + 1]
            entry = lax.broadcasted_iota(jnp.int32, (near, near + tok), 0)
            place = lax.broadcasted_iota(jnp.int32, (near, near + tok), 1)
            flip = (entry + place == near).astype(F32)
            line = jnp.dot(
                jnp.broadcast_to(table[:, :near], (8, near)), flip,
                preferred_element_type=F32, precision=lax.Precision.HIGHEST,
            )[:1]
            spot = lax.broadcasted_iota(jnp.int32, line.shape, 1)
            line = jnp.where((spot == 0) | (spot >= near), top, line)
            spread = jnp.broadcast_to(line, (tok, near + tok))
            row = lax.broadcasted_iota(jnp.int32, spread.shape, 0)
            step = 1
            while step < tok:
                moved = pltpu.roll(spread, step, 1)
                spread = jnp.where(lax.rem(row // step, 2) == 1, moved, spread)
                step *= 2
            far = jnp.broadcast_to(top, (tok, span - near))
            whole = jnp.concatenate([far, spread[:, :near]], axis=1)
            bias[layer] = jnp.where(live, whole, NEG_FILL)

        heads[1, :reach] = jnp.zeros((reach, head), BF16)
        heads[2, :reach] = jnp.zeros((reach, head), BF16)

        def attend(layer, b):
            qb = heads[0, trows(b, reach)]
            kb = heads[1, pl.ds(pl.multiple_of(b * tok, tok), span)]
            vb = heads[2, pl.ds(pl.multiple_of(b * tok, tok), span)]
            scores = lax.dot_general(
                qb, kb, (((1,), (1,)), ((), ())), preferred_element_type=F32
            ) * head ** (-0.5) + bias[layer]
            column = lax.broadcasted_iota(jnp.int32, scores.shape, 1)
            scores = jnp.where(column >= reach - b * tok, scores, NEG_FILL)
            e = jnp.exp(scores - jnp.max(scores, axis=-1, keepdims=True))
            e = (e * (1.0 / jnp.sum(e, axis=-1, keepdims=True))).astype(BF16)
            return jnp.dot(e, vb, preferred_element_type=F32).astype(BF16)

        def mix_z(layer, b):
            dst = mixed.at[layer, s, trows(lax.rem(b, 2))]
            return rcopy(
                own_mix.at[layer, b], dst, mzs.at[layer], mzr.at[layer, z], 2 * (b // 2) + y, t
            )

        def mix_y(layer, c):
            block = mixed.at[layer, 2 * c + y]
            return rcopy(block, block, mys.at[layer], myr.at[layer, c], side, t)

        def run_heads(layer, order, wait_block):
            def one(i, _):
                b = order(i)
                wait_block(b)
                result = attend(layer, b)

                @pl.when(b // 2 != z)
                def _():
                    own_mix[layer, b] = result
                    mix_z(layer, b).start()

                @pl.when(b // 2 == z)
                def _():
                    mixed[layer, s, trows(lax.rem(b, 2))] = result

                    @pl.when(lax.rem(b, 2) == 1)
                    def _():
                        mix_y(layer, z).start()

                return 0

            lax.fori_loop(0, n, one, 0)

        def forward_mix(layer):
            def one(i, _):
                c = near_level(i)
                arrived(mixed.at[layer, 2 * c + y], mzr.at[layer, c])
                mix_y(layer, c).start()
                return 0

            lax.fori_loop(1, levels, one, 0)

        def pcopy(layer, c):
            return rcopy(
                parts.at[layer, c, u], inbox.at[layer, c],
                ps.at[layer], pr.at[layer, c], s, u,
            )

        def bcopy(layer, c):
            return rcopy(
                joined.at[layer, c, v], branch.at[layer, y, c], bs.at[layer], br.at[layer], side, t
            )

        def project_branch(layer):
            for c in range(levels):
                arrived(mixed.at[layer, 2 * c + v], myr.at[layer, c])
            local[layer].wait()

            def project(c):
                @pl.when(c != z)
                def _():
                    arrived(out_half(layer, c, 1 - g), oxr.at[layer, c])

                lhs = jnp.concatenate([mixed[layer, j] for j in range(n)], axis=1)
                part = jnp.dot(lhs, outs[layer, c], preferred_element_type=F32).astype(BF16)
                for p in range(2):
                    for q in range(2):
                        parts[layer, c, q, p] = part[p * tok + q * share : p * tok + (q + 1) * share]
                pcopy(layer, c).start()

            def join(c):
                arrived(inbox.at[layer, c], pr.at[layer, c])
                both = parts[layer, c, t].astype(F32) + inbox[layer, c].astype(F32)
                joined[layer, c] = both.astype(BF16)
                bcopy(layer, c).start()
                branch[layer, y, c] = joined[layer, c, y]

            def step(i, _):
                project(near_level(i))

                @pl.when(i > 0)
                def _():
                    join(near_level(i - 1))

                return 0

            lax.fori_loop(0, levels, step, 0)
            join(near_level(levels - 1))
            arrived(branch.at[layer, v], br.at[layer])
            values = jnp.concatenate(
                [branch[layer, j % 2, j // 2] for j in range(n)], axis=1
            )
            return values.astype(F32)

        def branch_drain(layer):
            arrived(own_mix.at[layer, pl.ds(0, n - 2)], mzs.at[layer])
            arrived(mixed.at[layer, pl.ds(0, levels)], mys.at[layer])
            arrived(inbox.at[layer], ps.at[layer])
            arrived(branch.at[layer, 0], bs.at[layer])

        def heads_ready(b):
            arrived(heads.at[:, trows(b, reach)], hr.at[b])

        out_hop(0, 1)
        run_heads(0, lambda i: i, heads_ready)
        out_hop(0, 2)
        forward_mix(0)
        for k in range(1, n):
            for i in range(3):
                weight_copy(i, peer(k)).start()
        for d in range(3, levels):
            out_hop(0, d)
        values = project_branch(0)
        local[2].wait()
        hidden = (res[...].astype(F32) + scaled(values) * post1[...]).astype(BF16)
        res[...] = hidden
        rows2[2 * s + t] = (scaled(hidden.astype(F32)) * pre2[...]).astype(BF16)

        def piece_of(item, m):
            return rows2.at[item, :, pl.ds(pl.multiple_of(m * wide, wide), wide)]

        def row_z(c, m, to):
            block = piece_of(2 * (2 * c + y) + t, m)
            return rcopy(block, block, rzs, rzr.at[c, m], 2 * to + y, t)

        def row_y(c, m):
            block = piece_of(2 * (2 * c + y) + t, m)
            return rcopy(block, block, rys, ryr.at[c, m], side, t)

        def row_d(src, m):
            block = piece_of(2 * src + t, m)
            return rcopy(block, block, rds, rdr.at[src], s, u)

        def own_rows(m, _):
            @pl.when(z < levels - 1)
            def _():
                row_z(z, m, z + 1).start()

            @pl.when(z > 0)
            def _():
                row_z(z, m, z - 1).start()

            row_y(z, m).start()
            row_d(s, m).start()
            return 0

        lax.fori_loop(0, pieces, own_rows, 0)

        def hand_weights(k, _):
            src = peer(k)
            arrived(weight_half(src, g), wr.at[src, g])
            weight_hand(src).start()
            return 0

        lax.fori_loop(1, n, hand_weights, 0)

        def from_level(c, m, on, to):
            arrived(piece_of(2 * (2 * c + y) + t, m), rzr.at[c, m])

            @pl.when(on)
            def _():
                row_z(c, m, to).start()

            row_y(c, m).start()
            row_d(2 * c + y, m).start()

        def from_side(c, m):
            arrived(piece_of(2 * (2 * c + v) + t, m), ryr.at[c, m])
            row_d(2 * c + v, m).start()

        def rows_hop(d):
            def one(m, _):
                if d < levels:
                    @pl.when(z >= d)
                    def _():
                        from_level(z - d, m, z < levels - 1, z + 1)

                    @pl.when(z + d < levels)
                    def _():
                        from_level(z + d, m, z > 0, z - 1)

                if d == 1:
                    from_side(z, m)
                else:
                    @pl.when(z >= d - 1)
                    def _():
                        from_side(z - (d - 1), m)

                    @pl.when(z + d - 1 < levels)
                    def _():
                        from_side(z + (d - 1), m)

                return 0

            lax.fori_loop(0, pieces, one, 0)

        for d in range(1, levels + 1):
            rows_hop(d)
            if d == 1:
                out_start(1)
        out_hop(1, 1)

        def weights_ready(k, _):
            src = peer(k)
            arrived(weight_half(src, 1 - g), wr.at[src, 1 - g])
            return 0

        lax.fori_loop(1, n, weights_ready, 0)
        arrived(weights.at[pl.ds(pl.multiple_of(s * wrows, wrows), wrows)], wr.at[s, 0])

        def project_rows(i, _):
            c = near_level(i)
            arrived(rows2.at[4 * c + u], rdr.at[2 * c])
            arrived(rows2.at[4 * c + 2 + u], rdr.at[2 * c + 1])
            lhs = rows2[pl.ds(4 * c, 4)].reshape(2 * tok, width)
            both = jnp.dot(lhs, weights[...], preferred_element_type=F32).astype(BF16)
            start = pl.ds(pl.multiple_of(reach + c * 2 * tok, tok), 2 * tok)
            for i in range(3):
                heads[i, start] = both[:, i * head : (i + 1) * head]
            return 0

        lax.fori_loop(0, levels, project_rows, 0)
        for d in range(2, levels - 1):
            out_hop(1, d)
        run_heads(1, lambda i: lax.rem(2 * z + 2 + i, n), lambda b: None)
        forward_mix(1)
        if levels > 2:
            out_hop(1, levels - 1)
        values = project_branch(1)
        done = (res[...].astype(F32) + scaled(values) * post2[...]).astype(BF16)
        last[t] = done
        final = rcopy(last.at[t], last.at[t], fs, fr, s, u)
        final.start()

        arrived(heads.at[:, pl.ds(reach, (n - 1) * tok)], hs)
        arrived(weights.at[pl.ds(0, (n - 1) * hrows)], ws)
        arrived(weights.at[pl.ds(0, (n - 1) * hrows)], wf)
        for layer in range(2):
            out_drain(layer)
            branch_drain(layer)
        for at in range(levels):
            count = (1 + at if at < levels - 1 else 0) + (levels - at if at > 0 else 0)
            block = rows2.at[pl.ds(0, count)]

            @pl.when(z == at)
            def _():
                arrived(block, rzs)

        arrived(rows2.at[pl.ds(0, levels)], rys)
        arrived(rows2.at[pl.ds(0, n)], rds)
        final.wait_send()
        rcopy(last.at[u], last.at[u], fs, fr, s, u).wait_recv()
        out_ref[:share] = last[0]
        out_ref[share:] = last[1]

    dma = pltpu.SemaphoreType.DMA
    scratch = [
        pltpu.VMEM((3, reach + n * tok, head), BF16),
        pltpu.VMEM((width, 3 * head), BF16),
        pltpu.VMEM((2, levels, depth, cols), BF16),
        pltpu.VMEM((share, width), BF16),
        pltpu.VMEM((2, tok, span), F32),
        pltpu.VMEM((2, n, tok, head), BF16),
        pltpu.VMEM((2, n, 2 * tok, head), BF16),
        pltpu.VMEM((2, levels, 2, 2, share, cols), BF16),
        pltpu.VMEM((2, levels, 2, share, cols), BF16),
        pltpu.VMEM((2, levels, 2, share, cols), BF16),
        pltpu.VMEM((2, 2, levels, share, cols), BF16),
        pltpu.VMEM((2 * n, share, width), BF16),
        pltpu.VMEM((2, share, width), BF16),
        dma((3,)),
        dma, dma((n,)),
        dma, dma((n, 2)), dma,
        dma((2,)), dma((2, levels)), dma((2,)), dma((2, levels)),
        dma((2,)), dma((2, levels)), dma((2,)), dma((2, levels)),
        dma((2,)), dma((2, levels)), dma((2,)), dma((2,)),
        dma, dma((levels, pieces)), dma, dma((levels, pieces)), dma, dma((n,)),
        dma, dma,
    ]
    return kernel, scratch


def by_heads(
    resid, queries_first, keys_first, values_first, rel_first, post_first, out_first, pre_second,
    query_weight, key_weight, value_weight, rel_second, post_second, out_second,
):
    n = lax.axis_size("sp")
    tok, width = resid.shape
    head = queries_first.shape[1] // rel_first.shape[0]
    kernel, scratch = build_kernel(n, tok, head, width, REACH)
    hbm = pl.BlockSpec(memory_space=pltpu.HBM)
    vmem = pl.BlockSpec(memory_space=pltpu.VMEM)
    return pl.pallas_call(
        kernel,
        out_shape=jax.ShapeDtypeStruct((tok, width), BF16),
        in_specs=[hbm] * 9 + [vmem] * 5,
        out_specs=vmem,
        scratch_shapes=scratch,
        compiler_params=pltpu.CompilerParams(
            collective_id=0, has_side_effects=True, vmem_limit_bytes=60 * 2**20
        ),
    )(
        queries_first, keys_first, values_first, query_weight, key_weight, value_weight, resid,
        out_first, out_second, rel_first, rel_second,
        post_first[None], pre_second[None], post_second[None],
    )


def solution(mesh):
    in_specs = (
        P(("grp", "sp"), None),
        P(("grp", "sp"), "tp"),
        P(("grp", "sp"), "tp"),
        P(("grp", "sp"), "tp"),
        P("tp", None),
        P(),
        P("tp", "sp"),
        P(),
        P("sp", "tp"),
        P("sp", "tp"),
        P("sp", "tp"),
        P("tp", None),
        P(),
        P("tp", "sp"),
    )
    out_specs = P(("grp", "sp"), None)
    return jax.shard_map(shards, mesh=mesh, in_specs=in_specs, out_specs=out_specs, check_vma=False)
```

time: 145 us -> 120 us (0.83)
  the two profiles are of different devices: /device:TPU:27 before, /device:TPU:0 now
where the time goes in v1:
time: 120 us; the launch traced here: 119 us
  Pallas kernels  118 us (98%)
  local copies, waits for them, and re-layouts  1.88 us (2%)
    pallas_call x1, Pallas kernels, by_heads(): pl.pallas_call(kernel, out_shape=jax.ShapeDtypeStruct((tok, width), BF16)...  118 us

profile of v1, /device:TPU:0, one launch (start us, length us, event | category | flops | bytes accessed | tf_op | source)
XLA Modules:
  0.0 119.4 jit_solution(8454086471645122349)
XLA Ops:
  0.0 117.5 %shard_map.136 = bf16[128,2048]{1,0:T(8,128)(2,1)} custom-call(bf16[128,1024]{1,0:T(8,128)(2,1)} %q_hbm.1, bf16[128,1024]{1,0:T(8,128)(2,1)} %k_hbm.1, bf16[128,1024]{1,0:T(8,128)(2,1)} %v_hbm.1, bf16[256,1024]{1,0:T(8,128)(2,1)} %wq_hbm.1, bf16[256,1024]{1,0:T(8,128)(2,1)} %wk_hbm.1, bf16[256,1024]{1,0:T(8,128)(2,1)} %wv_hbm.1, ...), custom_call_target="tpu_custom_call" | custom-call | tf_op jit(solution)/shard_map/pallas_call | solution.py:682
  117.5 1.9 %copy.16 = bf16[128,2048]{1,0:T(8,128)(2,1)} copy(bf16[128,2048]{1,0:T(8,128)(2,1)} %shard_map.136) | data formatting | bytes 1048576

commit v2 on v1

--- a/solution.py
+++ b/solution.py
@@ -397,7 +397,7 @@
             block = mixed.at[layer, 2 * c + y]
             return rcopy(block, block, mys.at[layer], myr.at[layer, c], side, t)
 
-        def run_heads(layer, order, wait_block):
+        def one_head(layer, order, wait_block):
             def one(i, _):
                 b = order(i)
                 wait_block(b)
@@ -418,7 +418,7 @@
 
                 return 0
 
-            lax.fori_loop(0, n, one, 0)
+            return one
 
         def forward_mix(layer):
             def one(i, _):
@@ -491,7 +491,7 @@
             arrived(heads.at[:, trows(b, reach)], hr.at[b])
 
         out_hop(0, 1)
-        run_heads(0, lambda i: i, heads_ready)
+        lax.fori_loop(0, n, one_head(0, lambda i: i, heads_ready), 0)
         out_hop(0, 2)
         forward_mix(0)
         for k in range(1, n):
@@ -534,6 +534,7 @@
             return 0
 
         lax.fori_loop(0, pieces, own_rows, 0)
+        out_start(1)
 
         def hand_weights(k, _):
             src = peer(k)
@@ -583,22 +584,19 @@
 
             lax.fori_loop(0, pieces, one, 0)
 
-        for d in range(1, levels + 1):
-            rows_hop(d)
-            if d == 1:
-                out_start(1)
-        out_hop(1, 1)
+        def by_distance(i):
+            low = jnp.minimum(z, levels - 1 - z)
+            c = jnp.where(i <= low, low - i, i)
+            return jnp.where(2 * z < levels, c, levels - 1 - c)
 
         def weights_ready(k, _):
             src = peer(k)
             arrived(weight_half(src, 1 - g), wr.at[src, 1 - g])
             return 0
 
-        lax.fori_loop(1, n, weights_ready, 0)
-        arrived(weights.at[pl.ds(pl.multiple_of(s * wrows, wrows), wrows)], wr.at[s, 0])
 
         def project_rows(i, _):
-            c = near_level(i)
+            c = by_distance(i)
             arrived(rows2.at[4 * c + u], rdr.at[2 * c])
             arrived(rows2.at[4 * c + 2 + u], rdr.at[2 * c + 1])
             lhs = rows2[pl.ds(4 * c, 4)].reshape(2 * tok, width)
@@ -608,10 +606,29 @@
                 heads[i, start] = both[:, i * head : (i + 1) * head]
             return 0
 
-        lax.fori_loop(0, levels, project_rows, 0)
-        for d in range(2, levels - 1):
-            out_hop(1, d)
-        run_heads(1, lambda i: lax.rem(2 * z + 2 + i, n), lambda b: None)
+        def weights_here():
+            lax.fori_loop(1, n, weights_ready, 0)
+            arrived(weights.at[pl.ds(pl.multiple_of(s * wrows, wrows), wrows)], wr.at[s, 0])
+
+        lag = reach // tok
+        top = z == levels - 1
+        start = jnp.where(top, lag + 2, jnp.where(z == 0, 0, 2 * z + 2))
+        early = jnp.where(top, n - 2 - lag, jnp.where(z == 0, n - 2, n))
+        known = jnp.where(top | (z == 0), levels - 1, levels)
+        head_two = one_head(1, lambda i: lax.rem(start + i, n), lambda b: None)
+
+        for d in range(1, levels + 1):
+            rows_hop(d)
+            if d == 2:
+                out_hop(1, 1)
+                weights_here()
+                lax.fori_loop(0, 2, project_rows, 0)
+            if d == levels - 1:
+                out_hop(1, 2)
+                lax.fori_loop(2, known, project_rows, 0)
+                lax.fori_loop(0, early, head_two, 0)
+        lax.fori_loop(known, levels, project_rows, 0)
+        lax.fori_loop(early, n, head_two, 0)
         forward_mix(1)
         if levels > 2:
             out_hop(1, levels - 1)

time: 120 us -> 115 us (0.958)
  Pallas kernels: 118 us -> 113 us
    pallas_call x1, Pallas kernels: 118 us -> 113 us  [by_heads(): pl.pallas_call(kernel, out_shape=jax.ShapeDtypeStruct((tok, width), BF16)...]
where the time goes in v2:
time: 115 us
  Pallas kernels  113 us (98%)
  local copies, waits for them, and re-layouts  1.88 us (2%)
    pallas_call x1, Pallas kernels, by_heads(): pl.pallas_call(kernel, out_shape=jax.ShapeDtypeStruct((tok, width), BF16)...  113 us

profile of v2, /device:TPU:0, one launch (start us, length us, event | category | flops | bytes accessed | tf_op | source)
XLA Modules:
  0.0 114.8 jit_solution(11594691864525628861)
XLA Ops:
  0.0 112.9 %shard_map.136 = bf16[128,2048]{1,0:T(8,128)(2,1)} custom-call(bf16[128,1024]{1,0:T(8,128)(2,1)} %q_hbm.1, bf16[128,1024]{1,0:T(8,128)(2,1)} %k_hbm.1, bf16[128,1024]{1,0:T(8,128)(2,1)} %v_hbm.1, bf16[256,1024]{1,0:T(8,128)(2,1)} %wq_hbm.1, bf16[256,1024]{1,0:T(8,128)(2,1)} %wk_hbm.1, bf16[256,1024]{1,0:T(8,128)(2,1)} %wv_hbm.1, ...), custom_call_target="tpu_custom_call" | custom-call | tf_op jit(solution)/shard_map/pallas_call | solution.py:699
  112.9 1.9 %copy.16 = bf16[128,2048]{1,0:T(8,128)(2,1)} copy(bf16[128,2048]{1,0:T(8,128)(2,1)} %shard_map.136) | data formatting | bytes 1048576

commit v3 on v2

--- a/solution.py
+++ b/solution.py
@@ -186,6 +186,7 @@
     wrows = width // n
     hrows = wrows // 2
     pieces = 4
+    cuts = 2
     wide = width // pieces
 
     def kernel(
@@ -194,7 +195,7 @@
         out_ref,
         heads, weights, outs, res, bias, own_mix, mixed, parts, inbox, joined, branch, rows2, last,
         loc_sem, hs, hr, ws, wr, wf, mzs, mzr, mys, myr, ozs, ozr, oxs, oxr,
-        ps, pr, bs, br, rzs, rzr, rys, ryr, rds, rdr, fs, fr,
+        ms, mr, ns, nr, nxs, nxr, ps, pr, bs, br, rzs, rzr, rys, ryr, rds, rdr, fs, fr,
     ):
         s = lax.axis_index("sp")
         t = lax.axis_index("tp")
@@ -205,6 +206,9 @@
         v = 1 - y
         side = 2 * z + v
         turn = 1 - 2 * lax.rem(z, 2)
+        rung = lax.rem(z, 2)
+        twin = z + 1 - 2 * rung
+        across = lax.rem(z + levels // 2, levels)
 
         def rcopy(src, dst, ssem, rsem, sp, tp, grp=g):
             return pltpu.make_async_remote_copy(
@@ -217,6 +221,11 @@
 
         def near_level(i):
             return lax.rem(z + turn * i + levels, levels)
+
+        def by_distance(i):
+            low = jnp.minimum(z, levels - 1 - z)
+            c = jnp.where(i <= low, low - i, i)
+            return jnp.where(2 * z < levels, c, levels - 1 - c)
 
         def arrived(ref, sem):
             pltpu.make_async_copy(ref, ref, sem).wait()
@@ -242,7 +251,6 @@
 
         qkv = (q_hbm, k_hbm, v_hbm)
         wqkv = (wq_hbm, wk_hbm, wv_hbm)
-        out_hbm = (o1_hbm, o2_hbm)
 
         def head_copy(i, j):
             dst = heads.at[i, trows(s, reach)]
@@ -262,65 +270,97 @@
             piece = weight_half(src, g)
             return rcopy(piece, piece, wf, wr.at[src, g], s, t, 1 - g)
 
-        def out_half(layer, c, part):
-            return outs.at[layer, c, pl.ds(pl.multiple_of(part * dhalf, dhalf), dhalf)]
-
-        def out_own(layer, to):
-            piece = out_hbm[layer].at[pl.ds(pl.multiple_of(g * dhalf, dhalf), dhalf)]
-            return rcopy(
-                piece, out_half(layer, z, g), ozs.at[layer], ozr.at[layer, z], 2 * to + y, t
-            )
-
-        def out_pass(layer, c, to):
-            piece = out_half(layer, c, g)
-            return rcopy(piece, piece, ozs.at[layer], ozr.at[layer, c], 2 * to + y, t)
-
-        def out_hand(layer, c):
-            piece = out_half(layer, c, g)
-            return rcopy(piece, piece, oxs.at[layer], oxr.at[layer, c], s, t, 1 - g)
-
-        def out_start(layer):
-            @pl.when(z < levels - 1)
-            def _():
-                out_own(layer, z + 1).start()
-
-            @pl.when(z > 0)
-            def _():
-                out_own(layer, z - 1).start()
-
-        def out_hop(layer, d):
-            @pl.when(z >= d)
-            def _():
-                arrived(out_half(layer, z - d, g), ozr.at[layer, z - d])
-
+        dcut = dhalf // cuts
+
+        def out_half(c, part):
+            return outs.at[0, c, pl.ds(pl.multiple_of(part * dhalf, dhalf), dhalf)]
+
+        def out_piece(c, h):
+            return outs.at[0, c, pl.ds(pl.multiple_of(g * dhalf + h * dcut, dcut), dcut)]
+
+        def out_own(h, to):
+            piece = o1_hbm.at[pl.ds(pl.multiple_of(g * dhalf + h * dcut, dcut), dcut)]
+            return rcopy(piece, out_piece(z, h), ozs, ozr.at[z, h], 2 * to + y, t)
+
+        def out_pass(c, h, to):
+            piece = out_piece(c, h)
+            return rcopy(piece, piece, ozs, ozr.at[c, h], 2 * to + y, t)
+
+        def out_hand(c, h):
+            piece = out_piece(c, h)
+            return rcopy(piece, piece, oxs, oxr.at[c], s, t, 1 - g)
+
+        def out_start():
+            for h in range(cuts):
                 @pl.when(z < levels - 1)
                 def _():
-                    out_pass(layer, z - d, z + 1).start()
-
-                out_hand(layer, z - d).start()
-
-            @pl.when(z + d < levels)
-            def _():
-                arrived(out_half(layer, z + d, g), ozr.at[layer, z + d])
+                    out_own(h, z + 1).start()
 
                 @pl.when(z > 0)
                 def _():
-                    out_pass(layer, z + d, z - 1).start()
-
-                out_hand(layer, z + d).start()
-
-        def out_drain(layer):
+                    out_own(h, z - 1).start()
+
+        def out_hop(d):
+            for h in range(cuts):
+                @pl.when(z >= d)
+                def _():
+                    arrived(out_piece(z - d, h), ozr.at[z - d, h])
+
+                    @pl.when(z < levels - 1)
+                    def _():
+                        out_pass(z - d, h, z + 1).start()
+
+                    out_hand(z - d, h).start()
+
+                @pl.when(z + d < levels)
+                def _():
+                    arrived(out_piece(z + d, h), ozr.at[z + d, h])
+
+                    @pl.when(z > 0)
+                    def _():
+                        out_pass(z + d, h, z - 1).start()
+
+                    out_hand(z + d, h).start()
+
+        def two_half(e, part):
+            return outs.at[1, e, pl.ds(pl.multiple_of(part * dhalf, dhalf), dhalf)]
+
+        def two_own(e, sp):
+            piece = o2_hbm.at[pl.ds(pl.multiple_of(g * dhalf, dhalf), dhalf)]
+            return rcopy(piece, two_half(e, g), ns, nr.at[e], sp, t)
+
+        def two_side():
+            piece = two_half(2 + y, g)
+            return rcopy(piece, piece, ns, nr.at[2 + y], side, t)
+
+        def two_hand(e):
+            piece = two_half(e, g)
+            return rcopy(piece, piece, nxs, nxr.at[e], s, t, 1 - g)
+
+        def two_start():
+            two_own(2 + y, 2 * across + y).start()
+
+        def two_near():
+            arrived(two_half(2 + y, g), nr.at[2 + y])
+            two_side().start()
+            two_hand(2 + y).start()
+
+        def two_far():
+            arrived(two_half(2 + v, g), nr.at[2 + v])
+            two_hand(2 + v).start()
+
+        def out_drain():
             for at in range(levels):
                 count = (1 + at if at < levels - 1 else 0) + (levels - at if at > 0 else 0)
                 block = rows2.at[pl.ds(0, count)]
 
                 @pl.when(z == at)
                 def _():
-                    arrived(block, ozs.at[layer])
-
-            arrived(rows2.at[pl.ds(0, levels - 1)], oxs.at[layer])
-
-        out_start(0)
+                    arrived(block, ozs)
+
+            arrived(rows2.at[pl.ds(0, levels - 1)], oxs)
+
+        out_start()
         for k in range(1, n):
             for i in range(3):
                 head_copy(i, peer(k)).start()
@@ -334,9 +374,10 @@
                 weights.at[pl.ds(pl.multiple_of(s * wrows, wrows), wrows), pl.ds(i * head, head)],
                 wr.at[s, 0],
             ).start()
+        two_own(y, side).start()
         local = [
             pltpu.make_async_copy(o1_hbm, outs.at[0, z], loc_sem.at[0]),
-            pltpu.make_async_copy(o2_hbm, outs.at[1, z], loc_sem.at[1]),
+            pltpu.make_async_copy(o2_hbm, outs.at[1, y], loc_sem.at[1]),
             pltpu.make_async_copy(
                 resid_hbm.at[pl.ds(pl.multiple_of(t * share, share), share)], res, loc_sem.at[2]
             ),
@@ -429,6 +470,39 @@
 
             lax.fori_loop(1, levels, one, 0)
 
+        def two_copy(layer, b, level):
+            dst = mixed.at[layer, s, trows(lax.rem(b // 2, 2))]
+            return rcopy(
+                own_mix.at[layer, b], dst, ms, mr,
+                2 * level + lax.rem(b, 2), t,
+            )
+
+        def two_head(layer, order, wait_block):
+            def one(i, _):
+                b = order(i)
+                wait_block(b)
+                result = attend(layer, b)
+                own_mix[layer, b] = result
+                level = b // 2
+                other = level + 1 - 2 * lax.rem(level, 2)
+                mine = lax.rem(b, 2) == y
+
+                @pl.when(jnp.logical_not(mine & (level == z)))
+                def _():
+                    two_copy(layer, b, level).start()
+
+                @pl.when(jnp.logical_not(mine & (other == z)))
+                def _():
+                    two_copy(layer, b, other).start()
+
+                @pl.when(mine & (level // 2 == z // 2))
+                def _():
+                    mixed[layer, s, trows(lax.rem(level, 2))] = result
+
+                return 0
+
+            return one
+
         def pcopy(layer, c):
             return rcopy(
                 parts.at[layer, c, u], inbox.at[layer, c],
@@ -436,19 +510,33 @@
             )
 
         def bcopy(layer, c):
+            if layer == 0:
+                return rcopy(
+                    joined.at[layer, c, v], branch.at[layer, y, c], bs.at[layer], br.at[layer],
+                    side, t,
+                )
             return rcopy(
-                joined.at[layer, c, v], branch.at[layer, y, c], bs.at[layer], br.at[layer], side, t
+                joined.at[layer, c, 1 - rung], branch.at[layer, rung, c],
+                bs.at[layer], br.at[layer], 2 * twin + y, t,
             )
 
         def project_branch(layer):
-            for c in range(levels):
-                arrived(mixed.at[layer, 2 * c + v], myr.at[layer, c])
+            if layer == 0:
+                for c in range(levels):
+                    arrived(mixed.at[layer, 2 * c + v], myr.at[layer, c])
+                own_block, mine, order = z, y, near_level
+                hand_ready = lambda c: arrived(out_half(c, 1 - g), oxr.at[c])
+            else:
+                arrived(mixed.at[layer, pl.ds(0, n - 1)], mr)
+                own_block, mine = y, rung
+                order = lambda i: 2 * (i // 2) + lax.rem(y + i, 2)
+                hand_ready = lambda e: arrived(two_half(e, 1 - g), nxr.at[e])
             local[layer].wait()
 
             def project(c):
-                @pl.when(c != z)
-                def _():
-                    arrived(out_half(layer, c, 1 - g), oxr.at[layer, c])
+                @pl.when(c != own_block)
+                def _():
+                    hand_ready(c)
 
                 lhs = jnp.concatenate([mixed[layer, j] for j in range(n)], axis=1)
                 part = jnp.dot(lhs, outs[layer, c], preferred_element_type=F32).astype(BF16)
@@ -462,43 +550,51 @@
                 both = parts[layer, c, t].astype(F32) + inbox[layer, c].astype(F32)
                 joined[layer, c] = both.astype(BF16)
                 bcopy(layer, c).start()
-                branch[layer, y, c] = joined[layer, c, y]
+                branch[layer, mine, c] = joined[layer, c, mine]
 
             def step(i, _):
-                project(near_level(i))
+                project(order(i))
 
                 @pl.when(i > 0)
                 def _():
-                    join(near_level(i - 1))
+                    join(order(i - 1))
 
                 return 0
 
             lax.fori_loop(0, levels, step, 0)
-            join(near_level(levels - 1))
-            arrived(branch.at[layer, v], br.at[layer])
-            values = jnp.concatenate(
-                [branch[layer, j % 2, j // 2] for j in range(n)], axis=1
-            )
+            join(order(levels - 1))
+            arrived(branch.at[layer, 1 - mine], br.at[layer])
+
+            def column_block(j):
+                if layer == 0:
+                    return branch[layer, j % 2, j // 2]
+                half = lax.rem(j // levels + 2 * z // levels, 2)
+                return branch[layer, (j // 2) % 2, 2 * half + j % 2]
+
+            values = jnp.concatenate([column_block(j) for j in range(n)], axis=1)
             return values.astype(F32)
 
         def branch_drain(layer):
-            arrived(own_mix.at[layer, pl.ds(0, n - 2)], mzs.at[layer])
-            arrived(mixed.at[layer, pl.ds(0, levels)], mys.at[layer])
+            if layer == 0:
+                arrived(own_mix.at[layer, pl.ds(0, n - 2)], mzs.at[layer])
+                arrived(mixed.at[layer, pl.ds(0, levels)], mys.at[layer])
+            else:
+                arrived(mixed.at[layer, pl.ds(0, n - 1)], ms)
             arrived(inbox.at[layer], ps.at[layer])
             arrived(branch.at[layer, 0], bs.at[layer])
 
         def heads_ready(b):
             arrived(heads.at[:, trows(b, reach)], hr.at[b])
 
-        out_hop(0, 1)
+        out_hop(1)
         lax.fori_loop(0, n, one_head(0, lambda i: i, heads_ready), 0)
-        out_hop(0, 2)
+        out_hop(2)
         forward_mix(0)
         for k in range(1, n):
             for i in range(3):
                 weight_copy(i, peer(k)).start()
         for d in range(3, levels):
-            out_hop(0, d)
+            out_hop(d)
         values = project_branch(0)
         local[2].wait()
         hidden = (res[...].astype(F32) + scaled(values) * post1[...]).astype(BF16)
@@ -534,7 +630,7 @@
             return 0
 
         lax.fori_loop(0, pieces, own_rows, 0)
-        out_start(1)
+        two_start()
 
         def hand_weights(k, _):
             src = peer(k)
@@ -543,6 +639,8 @@
             return 0
 
         lax.fori_loop(1, n, hand_weights, 0)
+        arrived(two_half(v, g), nr.at[v])
+        two_hand(v).start()
 
         def from_level(c, m, on, to):
             arrived(piece_of(2 * (2 * c + y) + t, m), rzr.at[c, m])
@@ -583,11 +681,6 @@
                 return 0
 
             lax.fori_loop(0, pieces, one, 0)
-
-        def by_distance(i):
-            low = jnp.minimum(z, levels - 1 - z)
-            c = jnp.where(i <= low, low - i, i)
-            return jnp.where(2 * z < levels, c, levels - 1 - c)
 
         def weights_ready(k, _):
             src = peer(k)
@@ -615,23 +708,20 @@
         start = jnp.where(top, lag + 2, jnp.where(z == 0, 0, 2 * z + 2))
         early = jnp.where(top, n - 2 - lag, jnp.where(z == 0, n - 2, n))
         known = jnp.where(top | (z == 0), levels - 1, levels)
-        head_two = one_head(1, lambda i: lax.rem(start + i, n), lambda b: None)
+        head_two = two_head(1, lambda i: lax.rem(start + i, n), lambda b: None)
 
         for d in range(1, levels + 1):
             rows_hop(d)
             if d == 2:
-                out_hop(1, 1)
                 weights_here()
                 lax.fori_loop(0, 2, project_rows, 0)
             if d == levels - 1:
-                out_hop(1, 2)
+                two_near()
                 lax.fori_loop(2, known, project_rows, 0)
                 lax.fori_loop(0, early, head_two, 0)
         lax.fori_loop(known, levels, project_rows, 0)
         lax.fori_loop(early, n, head_two, 0)
-        forward_mix(1)
-        if levels > 2:
-            out_hop(1, levels - 1)
+        two_far()
         values = project_branch(1)
         done = (res[...].astype(F32) + scaled(values) * post2[...]).astype(BF16)
         last[t] = done
@@ -641,8 +731,10 @@
         arrived(heads.at[:, pl.ds(reach, (n - 1) * tok)], hs)
         arrived(weights.at[pl.ds(0, (n - 1) * hrows)], ws)
         arrived(weights.at[pl.ds(0, (n - 1) * hrows)], wf)
+        out_drain()
+        arrived(rows2.at[pl.ds(0, 3)], ns)
+        arrived(rows2.at[pl.ds(0, 3)], nxs)
         for layer in range(2):
-            out_drain(layer)
             branch_drain(layer)
         for at in range(levels):
             count = (1 + at if at < levels - 1 else 0) + (levels - at if at > 0 else 0)
@@ -677,8 +769,9 @@
         dma((3,)),
         dma, dma((n,)),
         dma, dma((n, 2)), dma,
-        dma((2,)), dma((2, levels)), dma((2,)), dma((2, levels)),
-        dma((2,)), dma((2, levels)), dma((2,)), dma((2, levels)),
+        dma((1,)), dma((1, levels)), dma((1,)), dma((1, levels)),
+        dma, dma((levels, cuts)), dma, dma((levels,)),
+        dma, dma, dma, dma((levels,)), dma, dma((levels,)),
         dma((2,)), dma((2, levels)), dma((2,)), dma((2,)),
         dma, dma((levels, pieces)), dma, dma((levels, pieces)), dma, dma((n,)),
         dma, dma,
@@ -698,7 +791,7 @@
     vmem = pl.BlockSpec(memory_space=pltpu.VMEM)
     return pl.pallas_call(
         kernel,
-        out_shape=jax.ShapeDtypeStruct((tok, width), BF16),
+        out_shape=pltpu.VMEM((tok, width), BF16),
         in_specs=[hbm] * 9 + [vmem] * 5,
         out_specs=vmem,
         scratch_shapes=scratch,

time: 115 us -> 111 us (0.965); the launches traced: 115 us -> 110 us
  Pallas kernels: 113 us -> 109 us
    pallas_call x1, Pallas kernels: 113 us -> 109 us  [by_heads(): pl.pallas_call(kernel, out_shape=pltpu.VMEM((tok, width), BF16), in_specs...]
where the time goes in v3:
time: 111 us; the launch traced here: 110 us
  Pallas kernels  109 us (98%)
    pallas_call x1, Pallas kernels, by_heads(): pl.pallas_call(kernel, out_shape=pltpu.VMEM((tok, width), BF16), in_specs...  109 us

profile of v3, /device:TPU:0, one launch (start us, length us, event | category | flops | bytes accessed | tf_op | source)
XLA Modules:
  0.0 109.6 jit_solution(4593516768379043167)
XLA Ops:
  0.0 108.8 %shard_map.136 = bf16[128,2048]{1,0:T(8,128)(2,1)S(1)} custom-call(bf16[128,1024]{1,0:T(8,128)(2,1)} %q_hbm.1, bf16[128,1024]{1,0:T(8,128)(2,1)} %k_hbm.1, bf16[128,1024]{1,0:T(8,128)(2,1)} %v_hbm.1, bf16[256,1024]{1,0:T(8,128)(2,1)} %wq_hbm.1, bf16[256,1024]{1,0:T(8,128)(2,1)} %wk_hbm.1, bf16[256,1024]{1,0:T(8,128)(2,1)} %wv_hbm.1, ...), custom_call_target="tpu_custom_call" | custom-call | tf_op jit(solution)/shard_map/pallas_call | solution.py:792
  108.8 0.8 copy.16

commit v4 on v3

--- a/solution.py
+++ b/solution.py
@@ -191,10 +191,11 @@
 
     def kernel(
         q_hbm, k_hbm, v_hbm, wq_hbm, wk_hbm, wv_hbm, resid_hbm, o1_hbm, o2_hbm,
+        rel1_hbm, rel2_hbm, post1_hbm, pre2_hbm, post2_hbm,
+        out_ref,
+        heads, weights, outs, res, bias, own_mix, mixed, parts, inbox, joined, branch, rows2,
         rel1, rel2, post1, pre2, post2,
-        out_ref,
-        heads, weights, outs, res, bias, own_mix, mixed, parts, inbox, joined, branch, rows2, last,
-        loc_sem, hs, hr, ws, wr, wf, mzs, mzr, mys, myr, ozs, ozr, oxs, oxr,
+        loc_sem, hs, hr, ws, wr, wf, wh, mzs, mzr, mys, myr, ozs, ozr, oxs, oxr,
         ms, mr, ns, nr, nxs, nxr, ps, pr, bs, br, rzs, rzr, rys, ryr, rds, rdr, fs, fr,
     ):
         s = lax.axis_index("sp")
@@ -230,6 +231,16 @@
         def arrived(ref, sem):
             pltpu.make_async_copy(ref, ref, sem).wait()
 
+        small = [
+            pltpu.make_async_copy(src, dst, loc_sem.at[3 + i])
+            for i, (src, dst) in enumerate(
+                ((rel1_hbm, rel1), (rel2_hbm, rel2), (post1_hbm, post1), (pre2_hbm, pre2),
+                 (post2_hbm, post2))
+            )
+        ]
+        for copy in small:
+            copy.start()
+
         barrier = pltpu.get_barrier_semaphore()
         for k in range(1, n):
             pl.semaphore_signal(
@@ -249,6 +260,13 @@
         def trows(j, base=0):
             return pl.ds(pl.multiple_of(base + j * tok, tok), tok)
 
+        def close(k):
+            return jnp.where(k == 0, side, jnp.where(k == 1, 2 * twin + y, 2 * twin + v))
+
+        def distant(k):
+            level = across + lax.rem(k // 2, 2) * (1 - 2 * lax.rem(across, 2))
+            return 2 * level + lax.rem(y + k, 2)
+
         qkv = (q_hbm, k_hbm, v_hbm)
         wqkv = (wq_hbm, wk_hbm, wv_hbm)
 
@@ -264,11 +282,11 @@
             start = pl.multiple_of(s * wrows + g * hrows, hrows)
             piece = wqkv[i].at[pl.ds(pl.multiple_of(g * hrows, hrows), hrows), lanes(j)]
             dst = weights.at[pl.ds(start, hrows), pl.ds(i * head, head)]
-            return rcopy(piece, dst, ws, wr.at[s, g], j, t)
+            return rcopy(piece, dst, ws, wr.at[s], j, t)
 
         def weight_hand(src):
             piece = weight_half(src, g)
-            return rcopy(piece, piece, wf, wr.at[src, g], s, t, 1 - g)
+            return rcopy(piece, piece, wf, wh, s, t, 1 - g)
 
         dcut = dhalf // cuts
 
@@ -361,9 +379,12 @@
             arrived(rows2.at[pl.ds(0, levels - 1)], oxs)
 
         out_start()
-        for k in range(1, n):
-            for i in range(3):
-                head_copy(i, peer(k)).start()
+        for i in range(3):
+            head_copy(i, side).start()
+        for a in range(1, levels):
+            for j in (y, v):
+                for i in range(3):
+                    head_copy(i, 2 * by_distance(a) + j).start()
         for i in range(3):
             pltpu.make_async_copy(
                 qkv[i].at[:, lanes(s)], heads.at[i, trows(s, reach)], hr.at[s]
@@ -372,9 +393,12 @@
             pltpu.make_async_copy(
                 wqkv[i].at[:, lanes(s)],
                 weights.at[pl.ds(pl.multiple_of(s * wrows, wrows), wrows), pl.ds(i * head, head)],
-                wr.at[s, 0],
+                wr.at[s],
             ).start()
         two_own(y, side).start()
+        for k in range(0, 3):
+            for i in range(3):
+                weight_copy(i, close(k)).start()
         local = [
             pltpu.make_async_copy(o1_hbm, outs.at[0, z], loc_sem.at[0]),
             pltpu.make_async_copy(o2_hbm, outs.at[1, y], loc_sem.at[1]),
@@ -385,6 +409,8 @@
         for copy in local:
             copy.start()
 
+        for copy in small:
+            copy.wait()
         near = 2 * REL_CLIP
         query = lax.broadcasted_iota(jnp.int32, (tok, span), 0) // SEG
         key = lax.broadcasted_iota(jnp.int32, (tok, span), 1) // SEG
@@ -583,6 +609,11 @@
             arrived(inbox.at[layer], ps.at[layer])
             arrived(branch.at[layer, 0], bs.at[layer])
 
+        def hand_weights(src):
+            arrived(weight_half(src, g), wr.at[src])
+            weight_hand(src).start()
+            return 0
+
         def heads_ready(b):
             arrived(heads.at[:, trows(b, reach)], hr.at[b])
 
@@ -590,11 +621,12 @@
         lax.fori_loop(0, n, one_head(0, lambda i: i, heads_ready), 0)
         out_hop(2)
         forward_mix(0)
-        for k in range(1, n):
+        for k in range(0, 4):
             for i in range(3):
-                weight_copy(i, peer(k)).start()
+                weight_copy(i, distant(k)).start()
         for d in range(3, levels):
             out_hop(d)
+        lax.fori_loop(0, 3, lambda k, c: hand_weights(close(k)), 0)
         values = project_branch(0)
         local[2].wait()
         hidden = (res[...].astype(F32) + scaled(values) * post1[...]).astype(BF16)
@@ -614,7 +646,7 @@
 
         def row_d(src, m):
             block = piece_of(2 * src + t, m)
-            return rcopy(block, block, rds, rdr.at[src], s, u)
+            return rcopy(block, block, rds, rdr.at[src // 2], s, u)
 
         def own_rows(m, _):
             @pl.when(z < levels - 1)
@@ -632,13 +664,7 @@
         lax.fori_loop(0, pieces, own_rows, 0)
         two_start()
 
-        def hand_weights(k, _):
-            src = peer(k)
-            arrived(weight_half(src, g), wr.at[src, g])
-            weight_hand(src).start()
-            return 0
-
-        lax.fori_loop(1, n, hand_weights, 0)
+        lax.fori_loop(0, 4, lambda k, c: hand_weights(distant(k)), 0)
         arrived(two_half(v, g), nr.at[v])
         two_hand(v).start()
 
@@ -682,16 +708,9 @@
 
             lax.fori_loop(0, pieces, one, 0)
 
-        def weights_ready(k, _):
-            src = peer(k)
-            arrived(weight_half(src, 1 - g), wr.at[src, 1 - g])
-            return 0
-
-
         def project_rows(i, _):
             c = by_distance(i)
-            arrived(rows2.at[4 * c + u], rdr.at[2 * c])
-            arrived(rows2.at[4 * c + 2 + u], rdr.at[2 * c + 1])
+            arrived(rows2.at[pl.ds(4 * c, 2)], rdr.at[c])
             lhs = rows2[pl.ds(4 * c, 4)].reshape(2 * tok, width)
             both = jnp.dot(lhs, weights[...], preferred_element_type=F32).astype(BF16)
             start = pl.ds(pl.multiple_of(reach + c * 2 * tok, tok), 2 * tok)
@@ -700,15 +719,20 @@
             return 0
 
         def weights_here():
-            lax.fori_loop(1, n, weights_ready, 0)
-            arrived(weights.at[pl.ds(pl.multiple_of(s * wrows, wrows), wrows)], wr.at[s, 0])
+            arrived(weights.at[pl.ds(0, (n - 1) * hrows)], wh)
+            arrived(weights.at[pl.ds(pl.multiple_of(s * wrows, wrows), wrows)], wr.at[s])
 
         lag = reach // tok
         top = z == levels - 1
-        start = jnp.where(top, lag + 2, jnp.where(z == 0, 0, 2 * z + 2))
         early = jnp.where(top, n - 2 - lag, jnp.where(z == 0, n - 2, n))
+        begin = jnp.where(top, lag + 2, jnp.where(2 * z < levels, lag, 0))
+
+        def two_order(i):
+            first = lax.rem(lag + i, n - 2)
+            return jnp.where(z == 0, jnp.where(i < n - 2, first, i), lax.rem(begin + i, n))
+
         known = jnp.where(top | (z == 0), levels - 1, levels)
-        head_two = two_head(1, lambda i: lax.rem(start + i, n), lambda b: None)
+        head_two = two_head(1, two_order, lambda b: None)
 
         for d in range(1, levels + 1):
             rows_hop(d)
@@ -724,8 +748,9 @@
         two_far()
         values = project_branch(1)
         done = (res[...].astype(F32) + scaled(values) * post2[...]).astype(BF16)
-        last[t] = done
-        final = rcopy(last.at[t], last.at[t], fs, fr, s, u)
+        mine_rows = out_ref.at[pl.ds(pl.multiple_of(t * share, share), share)]
+        mine_rows[...] = done
+        final = rcopy(mine_rows, mine_rows, fs, fr, s, u)
         final.start()
 
         arrived(heads.at[:, pl.ds(reach, (n - 1) * tok)], hs)
@@ -747,9 +772,8 @@
         arrived(rows2.at[pl.ds(0, levels)], rys)
         arrived(rows2.at[pl.ds(0, n)], rds)
         final.wait_send()
-        rcopy(last.at[u], last.at[u], fs, fr, s, u).wait_recv()
-        out_ref[:share] = last[0]
-        out_ref[share:] = last[1]
+        other_rows = out_ref.at[pl.ds(pl.multiple_of(u * share, share), share)]
+        rcopy(other_rows, other_rows, fs, fr, s, u).wait_recv()
 
     dma = pltpu.SemaphoreType.DMA
     scratch = [
@@ -765,15 +789,19 @@
         pltpu.VMEM((2, levels, 2, share, cols), BF16),
         pltpu.VMEM((2, 2, levels, share, cols), BF16),
         pltpu.VMEM((2 * n, share, width), BF16),
-        pltpu.VMEM((2, share, width), BF16),
-        dma((3,)),
+        pltpu.VMEM((n, 2 * REL_CLIP + 1), F32),
+        pltpu.VMEM((n, 2 * REL_CLIP + 1), F32),
+        pltpu.VMEM((1, width), F32),
+        pltpu.VMEM((1, width), F32),
+        pltpu.VMEM((1, width), F32),
+        dma((8,)),
         dma, dma((n,)),
-        dma, dma((n, 2)), dma,
+        dma, dma((n,)), dma, dma,
         dma((1,)), dma((1, levels)), dma((1,)), dma((1, levels)),
         dma, dma((levels, cuts)), dma, dma((levels,)),
         dma, dma, dma, dma((levels,)), dma, dma((levels,)),
         dma((2,)), dma((2, levels)), dma((2,)), dma((2,)),
-        dma, dma((levels, pieces)), dma, dma((levels, pieces)), dma, dma((n,)),
+        dma, dma((levels, pieces)), dma, dma((levels, pieces)), dma, dma((levels,)),
         dma, dma,
     ]
     return kernel, scratch
@@ -792,7 +820,7 @@
     return pl.pallas_call(
         kernel,
         out_shape=pltpu.VMEM((tok, width), BF16),
-        in_specs=[hbm] * 9 + [vmem] * 5,
+        in_specs=[hbm] * 14,
         out_specs=vmem,
         scratch_shapes=scratch,
         compiler_params=pltpu.CompilerParams(

time: 111 us -> 107 us (0.964); the launches traced: 110 us -> 107 us
  Pallas kernels: 109 us -> 106 us
    pallas_call x1, Pallas kernels: 109 us -> 106 us  [by_heads(): pl.pallas_call(kernel, out_shape=pltpu.VMEM((tok, width), BF16), in_specs...]
where the time goes in v4:
time: 107 us
  Pallas kernels  106 us (99%)
    pallas_call x1, Pallas kernels, by_heads(): pl.pallas_call(kernel, out_shape=pltpu.VMEM((tok, width), BF16), in_specs...  106 us

profile of v4, /device:TPU:0, one launch (start us, length us, event | category | flops | bytes accessed | tf_op | source)
XLA Modules:
  0.0 107.1 jit_solution(13117636794304524331)
XLA Ops:
  0.0 106.3 %shard_map.136 = bf16[128,2048]{1,0:T(8,128)(2,1)S(1)} custom-call(bf16[128,1024]{1,0:T(8,128)(2,1)} %q_hbm.1, bf16[128,1024]{1,0:T(8,128)(2,1)} %k_hbm.1, bf16[128,1024]{1,0:T(8,128)(2,1)} %v_hbm.1, bf16[256,1024]{1,0:T(8,128)(2,1)} %wq_hbm.1, bf16[256,1024]{1,0:T(8,128)(2,1)} %wk_hbm.1, bf16[256,1024]{1,0:T(8,128)(2,1)} %wv_hbm.1, ...), custom_call_target="tpu_custom_call" | custom-call | tf_op jit(solution)/shard_map/pallas_call | solution.py:820
  106.3 0.8 copy.16

commit v5 on v4

--- a/solution.py
+++ b/solution.py
@@ -619,6 +619,7 @@
 
         out_hop(1)
         lax.fori_loop(0, n, one_head(0, lambda i: i, heads_ready), 0)
+        lax.fori_loop(0, 3, lambda k, c: hand_weights(close(k)), 0)
         out_hop(2)
         forward_mix(0)
         for k in range(0, 4):
@@ -626,7 +627,6 @@
                 weight_copy(i, distant(k)).start()
         for d in range(3, levels):
             out_hop(d)
-        lax.fori_loop(0, 3, lambda k, c: hand_weights(close(k)), 0)
         values = project_branch(0)
         local[2].wait()
         hidden = (res[...].astype(F32) + scaled(values) * post1[...]).astype(BF16)
@@ -657,11 +657,15 @@
             def _():
                 row_z(z, m, z - 1).start()
 
+            return 0
+
+        def own_beside(m, _):
             row_y(z, m).start()
             row_d(s, m).start()
             return 0
 
         lax.fori_loop(0, pieces, own_rows, 0)
+        lax.fori_loop(0, pieces, own_beside, 0)
         two_start()
 
         lax.fori_loop(0, 4, lambda k, c: hand_weights(distant(k)), 0)

time: 107 us -> 107 us (level)
  no operation moved by 1% of the time
where the time goes in v5:
time: 107 us
  Pallas kernels  106 us (99%)
    pallas_call x1, Pallas kernels, by_heads(): pl.pallas_call(kernel, out_shape=pltpu.VMEM((tok, width), BF16), in_specs...  106 us

profile of v5, /device:TPU:0, one launch (start us, length us, event | category | flops | bytes accessed | tf_op | source)
XLA Modules:
  0.0 107.1 jit_solution(13259735360498118900)
XLA Ops:
  0.0 106.3 %shard_map.136 = bf16[128,2048]{1,0:T(8,128)(2,1)S(1)} custom-call(bf16[128,1024]{1,0:T(8,128)(2,1)} %q_hbm.1, bf16[128,1024]{1,0:T(8,128)(2,1)} %k_hbm.1, bf16[128,1024]{1,0:T(8,128)(2,1)} %v_hbm.1, bf16[256,1024]{1,0:T(8,128)(2,1)} %wq_hbm.1, bf16[256,1024]{1,0:T(8,128)(2,1)} %wk_hbm.1, bf16[256,1024]{1,0:T(8,128)(2,1)} %wv_hbm.1, ...), custom_call_target="tpu_custom_call" | custom-call | tf_op jit(solution)/shard_map/pallas_call | solution.py:824
  106.3 0.8 copy.16
